TPU v7x, 32 devices: a whole 2x2x4 slice. The times are simulated.
32 devices in a mesh: sp: 8 (over z, x), tp: 4 (over y, core).
Axes of the slice: x: 2, y: 2, z: 4, core: 2. Of those that a mesh axis runs over, the one named last changes fastest.
Arguments:
- residual: bfloat16 [1536, 2048], P('sp', 'tp'), may hold values from -10 to 10
- queries: bfloat16 [1536, 16, 128], P('sp', 'tp'), may hold values from -6.5 to 6.5
- key_rows: bfloat16 [1536, 16, 128], P('sp', 'tp'), may hold values from -6.5 to 6.5
- value_rows: bfloat16 [1536, 16, 128], P('sp', 'tp'), may hold values from -6 to 6
- diff_scale: float32 [16], P('tp'), may hold values from 0.3 to 0.8
- head_gain: float32 [128], replicated, may hold values from 0.1 to 1.9
- out_weight: bfloat16 [2048, 2048], P(None, 'tp'), may hold values from -0.125 to 0.125
- norm_gain: float32 [2048], replicated, may hold values from 0.1 to 1.9
- gate_weight: bfloat16 [8, 2048, 4096], P('sp', None, 'tp'), may hold values from -0.5 to 0.5
- up_weight: bfloat16 [8, 2048, 4096], P('sp', None, 'tp'), may hold values from -0.5 to 0.5
- down_weight: bfloat16 [8, 4096, 2048], P('sp', None, 'tp'), may hold values from -0.01171875 to 0.01171875
- expert_ids: int32 [1536, 2], P('sp'), may hold values from 0 to 7, all different within a row; in each aligned block of 192 rows (0 to 191, 192 to 383, ...) at most 96 rows name the same one
- route_logit: float32 [1536, 2], P('sp'), may hold values from -6 to 6
Outputs:
- updated: bfloat16 [1536, 2048], P('sp', 'tp')
Inputs may be any that keep to these rules, and one draw needn't show every extreme that they name: `expert_ids`: A token's 2 experts differ. The 192 tokens of one index of sp name one expert at most 96 times, a bound that some block reaches on some index.
All inputs are finite; a program needn't handle non-finite values.
Results may differ from a plain program's by a relative error of at most 0.014.
Values may be sent and summed in bfloat16 or wider, within the bound.
A program may use at most 64 MiB of HBM per device.

v0:
```python
import math
import jax
import jax.numpy as jnp
from jax import lax
from jax.sharding import PartitionSpec as P

D = 2048
QK = 64
SPAN = 64
NORM_EPS = 1e-05
CLAMP_LIMIT = 7.0
SWISH_ALPHA = 1.702
HEAD_KEEP = 0.8
NEG_FILL = -1e30


def update_map(running, query_half, key_half, value_block, visible):
    row_peak, row_total, accum = running
    scores = jnp.einsum(
        "qhd,khd->hqk", query_half, key_half, preferred_element_type=jnp.float32
    ) * QK ** (-0.5)
    scores = jnp.where(visible[None], scores, NEG_FILL)
    new_peak = jnp.maximum(row_peak, jnp.max(scores, axis=-1))
    exp_weights = jnp.where(visible[None], jnp.exp(scores - new_peak[..., None]), 0.0)
    rescale = jnp.exp(row_peak - new_peak)
    row_total = row_total * rescale + jnp.sum(exp_weights, axis=-1)
    accum = accum * rescale[..., None] + jnp.einsum(
        "hqk,khv->hqv",
        exp_weights.astype(jnp.bfloat16),
        value_block,
        preferred_element_type=jnp.float32,
    )
    return (new_peak, row_total, accum)


def local(
    residual,
    queries,
    key_rows,
    value_rows,
    diff_scale,
    head_gain,
    out_weight,
    norm_gain,
    gate_weight,
    up_weight,
    down_weight,
    expert_ids,
    route_logit,
):
    tokens_here = queries.shape[0]
    heads_here = queries.shape[1]
    value_width = value_rows.shape[2]
    query_start = lax.axis_index("sp") * tokens_here
    query_span = (query_start + jnp.arange(tokens_here, dtype=jnp.int32)) // SPAN
    first_query = queries[..., :QK]
    second_query = queries[..., QK:]
    empty_map = (
        jnp.full((heads_here, tokens_here), NEG_FILL, jnp.float32),
        jnp.zeros((heads_here, tokens_here), jnp.float32),
        jnp.zeros((heads_here, tokens_here, value_width), jnp.float32),
    )
    folded = (empty_map, empty_map)
    key_piece = lax.all_gather(key_rows, "sp", axis=0, tiled=True)
    value_piece = lax.all_gather(value_rows, "sp", axis=0, tiled=True)
    key_count = key_piece.shape[0]
    key_width = math.gcd(key_count, 1024)
    blocks = key_count // key_width
    key_blocks = key_piece.reshape(blocks, key_width, heads_here, 2 * QK)
    value_blocks = value_piece.reshape(blocks, key_width, heads_here, value_width)

    def advance(running, inputs):
        block_index, key_block, value_block = inputs
        key_start = block_index * key_width

        def compute(current):
            key_span = (key_start + jnp.arange(key_width, dtype=jnp.int32)) // SPAN
            visible = key_span[None, :] <= query_span[:, None]
            first = update_map(current[0], first_query, key_block[..., :QK], value_block, visible)
            second = update_map(current[1], second_query, key_block[..., QK:], value_block, visible)
            return (first, second)

        running = lax.cond(
            key_start < query_start + tokens_here, compute, lambda current: current, running
        )
        return (running, None)

    folded, _ = lax.scan(
        advance, folded, (jnp.arange(blocks, dtype=jnp.int32), key_blocks, value_blocks)
    )
    first_map, second_map = folded
    mixture = (
        first_map[2] / first_map[1][..., None]
        - diff_scale[:, None, None] * second_map[2] / second_map[1][..., None]
    )
    scale_back = lax.rsqrt(jnp.mean(mixture * mixture, axis=-1, keepdims=True) + NORM_EPS)
    attended = (mixture * scale_back * head_gain * HEAD_KEEP).astype(jnp.bfloat16)
    column_width = out_weight.shape[1]
    head_weight = out_weight.reshape(-1, value_width, column_width)
    weight_slice = head_weight
    projected = jnp.einsum(
        "htv,hvd->td",
        lax.all_gather(attended, "tp", axis=0, tiled=True),
        weight_slice,
        preferred_element_type=jnp.float32,
    )
    after_mixer = (residual.astype(jnp.float32) + projected).astype(jnp.bfloat16)
    mixer_float = after_mixer.astype(jnp.float32)
    partial_value = jnp.sum(mixer_float * mixer_float, axis=-1)
    square_total = lax.psum(partial_value, "tp")
    gain_slice = lax.dynamic_slice_in_dim(
        norm_gain, lax.axis_index("tp") * column_width, column_width, 0
    )
    normed = (mixer_float * lax.rsqrt(square_total / D + NORM_EPS)[:, None] * gain_slice).astype(
        jnp.bfloat16
    )
    experts = lax.axis_size("sp")
    top_count = expert_ids.shape[1]
    capacity = 2 * tokens_here * top_count // experts
    chosen = expert_ids.reshape(-1)
    onehot = (chosen[:, None] == jnp.arange(experts, dtype=jnp.int32)[None, :]).astype(jnp.int32)
    rank_in = jnp.sum(jnp.cumsum(onehot, axis=0) * onehot, axis=1) - 1
    slot_index = chosen * capacity + rank_in
    owner_row = (
        jnp.full((experts * capacity,), tokens_here, jnp.int32)
        .at[slot_index]
        .set(jnp.arange(tokens_here * top_count, dtype=jnp.int32) // top_count)
    )
    padded = jnp.concatenate([normed, jnp.zeros((1, normed.shape[1]), jnp.bfloat16)], axis=0)
    outgoing = padded[owner_row].reshape(experts, capacity, normed.shape[1])
    expert_input = lax.all_gather(
        lax.all_to_all(outgoing, "sp", split_axis=0, concat_axis=0, tiled=True),
        "tp",
        axis=2,
        tiled=True,
    )
    sources = expert_input.shape[0]
    items = expert_input.shape[1]
    flat_rows = expert_input.reshape(sources * items, -1)
    pre_gate = jnp.dot(flat_rows, gate_weight[0], preferred_element_type=jnp.float32)
    pre_up = jnp.dot(flat_rows, up_weight[0], preferred_element_type=jnp.float32)
    capped = jnp.minimum(pre_gate, CLAMP_LIMIT)
    linear = jnp.clip(pre_up, -CLAMP_LIMIT, CLAMP_LIMIT)
    hidden = (capped * jax.nn.sigmoid(SWISH_ALPHA * capped) * (linear + 1.0)).astype(jnp.bfloat16)
    weight_slice = down_weight[0]
    expert_out = jnp.dot(
        lax.all_gather(hidden, "tp", axis=1, tiled=True),
        weight_slice,
        preferred_element_type=jnp.float32,
    )
    expert_out = expert_out.astype(jnp.bfloat16).reshape(sources, items, -1)
    returned_rows = lax.all_to_all(expert_out, "sp", split_axis=0, concat_axis=0, tiled=True)
    picked = returned_rows.reshape(experts * capacity, -1)[slot_index].astype(jnp.float32)
    picked = picked.reshape(tokens_here, top_count, -1)
    weights = jax.nn.softmax(route_logit, axis=-1)
    routed = jnp.sum(picked * weights[..., None], axis=1)
    return (mixer_float + routed).astype(jnp.bfloat16)


def solution(mesh):
    return jax.shard_map(
        local,
        mesh=mesh,
        in_specs=(
            P("sp", "tp"),
            P("sp", "tp", None),
            P("sp", "tp", None),
            P("sp", "tp", None),
            P("tp"),
            P(),
            P(None, "tp"),
            P(),
            P("sp", None, "tp"),
            P("sp", None, "tp"),
            P("sp", None, "tp"),
            P("sp", None),
            P("sp", None),
        ),
        out_specs=P("sp", "tp"),
        check_vma=False,
    )
```

profile of v0, /device:TPU:0, one launch (start us, length us, event | category | flops | bytes accessed | tf_op | source)
XLA Modules:
  0.0 296.3 jit_solution(3500172858010482587)
XLA Ops:
  6.5 1.8 copy.27
  8.4 0.0 all-gather.5.cloned.1.call-update
  8.4 0.0 all-gather.7.cloned.1.call-start
  8.4 1.6 copy.29
  10.1 0.0 all-gather.7.cloned.1.call-update
  10.1 0.0 all-gather.9.cloned.1.call-start
  10.1 0.8 copy.34
  10.9 0.1 eq.29
  11.1 0.1 eq.25
  11.2 0.0 copy-done.2
  11.2 0.2 fusion.56
  11.4 0.1 copy.37
  11.6 0.1 copy.38
  11.8 0.9 reduce-window.6
  12.6 0.2 slice_reduce_fusion
  12.9 0.1 copy.33
  13.0 0.1 mul.173
  13.2 0.8 dynamic_slice.28
  14.0 0.1 fusion.44
  14.1 2.9 scatter_custom_fusion
  17.0 39.5 %all-gather.5.cloned.1.call-done = bf16[1536,4,128]{2,0,1:T(8,128)(2,1)} async-done(((bf16[192,4,128]{2,0,1:T(8,128)(2,1)}), bf16[1536,4,128]{2,0,1:T(8,128)(2,1)}) %all-gather.5.cloned.1.call-update) | async-done | bytes 1572880 | tf_op jit(solution)/shard_map/all_gather | solution.py:64
  56.5 2.6 copy.31
  59.1 42.2 %all-gather.7.cloned.1.call-done = bf16[1536,4,128]{2,0,1:T(8,128)(2,1)} async-done(((bf16[192,4,128]{2,0,1:T(8,128)(2,1)}), bf16[1536,4,128]{2,0,1:T(8,128)(2,1)}) %all-gather.7.cloned.1.call-update) | async-done | bytes 1572880 | tf_op jit(solution)/shard_map/all_gather | solution.py:65
  101.2 2.7 copy.32
  104.0 0.0 copy-start.6
  104.0 0.0 copy-start.7
  104.0 9.0 %while.23 = (s32[]{:T(128)}, f32[4,192]{1,0:T(4,128)S(1)}, f32[4,192]{1,0:T(4,128)S(1)}, f32[4,192,128]{2,1,0:T(8,128)S(1)}, f32[4,192]{1,0:T(4,128)S(1)}, /*ind...) while((s32[]{:T(128)}, f32[4,192]{1,0:T(4,128)S(1)}, ...), condition=%wide.region_7.8_spmd.clone, body=%wide.region_0.7_spmd.clone.sunk | while | flops 309574784 | bytes 20891532 | solution.py:88
  104.1 0.6 dynamic_slice.42
  105.4 5.0 %conditional.3 = ((f32[4,192]{1,0:T(4,128)S(1)}, f32[4,192]{1,0:T(4,128)S(1)}, f32[4,192,128]{2,1,0:T(8,128)S(1)}, f32[4,192]{1,0:T(4,128)S(1)}, f32[4,192]{1,0:T(4,128)S(1)}, /*index=5*/f32[4,192,128]{2,1,0:T(8,128)S(1)})) conditional(s32[]{:T(128)} %convert_element_type.82, (f32[4,192]{1,0:T(4,128)S(1)}, f32[4,192]{1,0:T(4,128)S(1)}, ...), branch_computations={%region_1.1_spmd, %region_2.6_spmd.clone} | conditional | flops 309572096 | bytes 20887848 | solution.py:83
  105.4 0.1 broadcast_compare_fusion
  105.5 1.1 dynamic-slice_bitcast_fusion
  106.6 0.6 fusion.54
  107.2 0.6 fusion.55
  107.8 1.2 fusion.5
  109.0 0.2 copy-done.1
  109.2 0.6 convolution_add_fusion
  109.7 0.6 convolution_add_fusion.1
  110.4 0.6 dynamic_slice.42
  111.7 0.6 dynamic_slice.42
  113.0 0.0 copy-start.3
  113.1 0.5 multiply_reduce_fusion.2
  113.6 0.2 multiply_convert_fusion.2
  113.7 8.6 %all_gather.17 = bf16[16,192,128]{2,1,0:T(8,128)(2,1)S(1)} all-gather(bf16[4,192,128]{2,1,0:T(8,128)(2,1)S(1)} %multiply_convert_fusion.2), channel_id=1, replica_groups=mesh['sp'=8,'tp'=4] {'tp'}, dimensions={0}, use_global_device_ids=true | all-gather | bytes 983040 | tf_op jit(solution)/shard_map/all_gather | solution.py:103
  122.3 0.0 copy-done.3
  122.3 0.7 multiply_reduce_fusion.1
  123.0 6.2 %psum.7 = f32[192]{0:T(256)S(1)} all-reduce(f32[192]{0:T(256)S(1)} %get-tuple-element.467), channel_id=1, replica_groups=mesh['sp'=8,'tp'=4] {'tp'}, use_global_device_ids=true, to_apply=%region_10.11 | all-reduce | flops 192 | bytes 1536 | tf_op jit(solution)/shard_map/psum | solution.py:110
  129.2 0.1 multiply_convert_fusion.1
  129.3 2.7 gather_fusion
  132.0 32.5 %all_to_all.10 = bf16[8,96,512]{2,1,0:T(8,128)(2,1)} all-to-all(bf16[8,96,512]{2,1,0:T(8,128)(2,1)S(1)} %bitcast.62), channel_id=1, replica_groups=mesh['sp'=8,'tp'=4] {'sp'}, dimensions={0} | all-to-all | bytes 1572864 | tf_op jit(solution)/shard_map/all_to_all | solution.py:132
  164.5 0.0 all-gather.9.cloned.1.call-update
  164.5 0.2 all-gather.11.cloned.1.call-start
  164.7 26.5 %all-gather.9.cloned.1.call-done = bf16[8,96,2048]{2,1,0:T(8,128)(2,1)} async-done(((bf16[8,96,512]{2,1,0:T(8,128)(2,1)}), bf16[8,96,2048]{2,1,0:T(8,128)(2,1)}) %all-gather.9.cloned.1.call-update) | async-done | bytes 3145744 | tf_op jit(solution)/shard_map/all_gather | solution.py:131
  191.3 6.3 %fusion.32 = f32[768,1024]{1,0:T(8,128)S(1)} fusion(bf16[768,2048]{1,0:T(8,128)(2,1)} %bitcast.67, bf16[1,2048,1024]{2,1,0:T(8,128)(2,1)} %param.26), kind=kOutput, calls=%fused_computation.55 | convolution fusion | flops 3221225472 | bytes 10485760 | tf_op jit(solution)/shard_map/dot_general | solution.py:141
  197.6 5.3 %multiply_convert_fusion = bf16[768,1024]{1,0:T(8,128)(2,1)} fusion(f32[768,1024]{1,0:T(8,128)S(1)} %fusion.32, bf16[768,2048]{1,0:T(8,128)(2,1)S(1)} %bitcast.68, bf16[1,2048,1024]{2,1,0:T(8,128)(2,1)S(1)} %copy-done.8), kind=kOutput, calls=%fused_computation.59 | convolution fusion | flops 3229089792 | bytes 12058624 | tf_op jit(solution)/shard_map/dot_general | solution.py:140
  202.9 0.0 all-gather.11.cloned.1.call-update
  202.9 46.5 %all-gather.11.cloned.1.call-done = bf16[768,4096]{1,0:T(8,128)(2,1)} async-done(((bf16[768,1024]{1,0:T(8,128)(2,1)}), bf16[768,4096]{1,0:T(8,128)(2,1)}) %all-gather.11.cloned.1.call-update) | async-done | bytes 6291472 | tf_op jit(solution)/shard_map/all_gather | solution.py:147
  249.4 8.3 %fusion.38 = bf16[768,512]{1,0:T(8,128)(2,1)} fusion(bf16[768,4096]{1,0:T(8,128)(2,1)} %all-gather.11.cloned.1.call-done, bf16[1,4096,512]{2,1,0:T(8,128)(2,1)} %param.27), kind=kOutput, calls=%fused_computation.60 | convolution fusion | flops 3221618688 | bytes 11272192 | tf_op jit(solution)/shard_map/dot_general | solution.py:146
  257.7 5.6 %all-to-all-start.1 = ((bf16[8,96,512]{2,1,0:T(8,128)(2,1)}), bf16[8,96,512]{2,1,0:T(8,128)(2,1)S(1)}, u32[]{:S(2)}, u32[]{:S(2)}) async-start(bf16[8,96,512]{2,1,0:T(8,128)(2,1)} %bitcast.65), calls=%async_computation.1 | async-start | bytes 1572864 | tf_op jit(solution)/shard_map/all_to_all | solution.py:152
  263.4 0.1 copy.36
  263.6 20.4 %all-to-all-done.1 = bf16[8,96,512]{2,1,0:T(8,128)(2,1)S(1)} async-done(((bf16[8,96,512]{2,1,0:T(8,128)(2,1)}), bf16[8,96,512]{2,1,0:T(8,128)(2,1)S(1)}, u32[]{:S(2)}, u32[]{:S(2)}) %all-to-all-start.1) | async-done | bytes 786464 | tf_op jit(solution)/shard_map/all_to_all | solution.py:152
  283.9 2.6 gather_fusion.1
  286.5 1.5 reshape.153
  288.0 1.0 multiply_reduce_fusion
  289.0 0.7 add_convert_fusion
  (58 shorter events, 0.4 us)
Async XLA Ops:
  6.5 115.8 %copy-start = (bf16[2048,512]{1,0:T(8,128)(2,1)S(1)}, bf16[2048,512]{1,0:T(8,128)(2,1)}, u32[]{:S(2)}) copy-start(bf16[2048,512]{1,0:T(8,128)(2,1)} %param.23) | copy-start | bytes 6291460
  6.5 6.4 %copy-start.5 = (s32[192,2]{0,1:T(2,128)S(1)}, s32[192,2]{0,1:T(2,128)}, u32[]{:S(2)}) copy-start(s32[192,2]{0,1:T(2,128)} %param.28) | copy-start | bytes 4612
  6.5 4.7 %copy-start.2 = (bf16[192,4,128]{2,1,0:T(4,128)(2,1)S(1)}, bf16[192,4,128]{2,1,0:T(4,128)(2,1)}, u32[]{:S(2)}) copy-start(bf16[192,4,128]{2,1,0:T(4,128)(2,1)} %param.18) | copy-start | bytes 589828
  6.5 49.9 %all-gather.5.cloned.1.call-start = ((), (), s32[]{:S(2)}) async-start(), calls=%async_computation.2 | async-start | bytes 1769472 | tf_op jit(solution)/shard_map/all_gather | solution.py:64
  8.4 92.9 %all-gather.7.cloned.1.call-start = ((), (), s32[]{:S(2)}) async-start(), calls=%async_computation.3 | async-start | bytes 1769472 | tf_op jit(solution)/shard_map/all_gather | solution.py:65
  10.1 181.2 %all-gather.9.cloned.1.call-start = ((), (), s32[]{:S(2)}) async-start(), calls=%async_computation.4 | async-start | bytes 3932160 | tf_op jit(solution)/shard_map/all_gather | solution.py:131
  104.0 9.0 %copy-start.6 = (f32[4]{0:T(128)S(1)}, f32[4]{0:T(128)}, u32[]{:S(2)}) copy-start(f32[4]{0:T(128)} %param.21) | copy-start | bytes 52
  104.0 9.5 %copy-start.7 = (f32[128]{0:T(128)S(1)}, f32[128]{0:T(128)}, u32[]{:S(2)}) copy-start(f32[128]{0:T(128)} %param.22) | copy-start | bytes 1540
  107.8 1.4 copy-start.1
  113.0 9.3 %copy-start.3 = (bf16[192,512]{1,0:T(8,128)(2,1)S(1)}, bf16[192,512]{1,0:T(8,128)(2,1)}, u32[]{:S(2)}) copy-start(bf16[192,512]{1,0:T(8,128)(2,1)} %param.17) | copy-start | bytes 589828
  164.5 84.9 %all-gather.11.cloned.1.call-start = ((), (), s32[]{:S(2)}) async-start(), calls=%async_computation.5 | async-start | bytes 7864320 | tf_op jit(solution)/shard_map/all_gather | solution.py:147
  191.2 6.3 %copy-start.8 = (bf16[1,2048,1024]{2,1,0:T(8,128)(2,1)S(1)}, bf16[1,2048,1024]{2,1,0:T(8,128)(2,1)}, u32[]{:S(2)}) copy-start(bf16[1,2048,1024]{2,1,0:T(8,128)(2,1)} %param.25) | copy-start | bytes 12582916
  191.3 6.3 %copy-start.9 = (bf16[8,96,2048]{2,1,0:T(8,128)(2,1)S(1)}, bf16[8,96,2048]{2,1,0:T(8,128)(2,1)}, u32[]{:S(2)}) copy-start(bf16[8,96,2048]{2,1,0:T(8,128)(2,1)} %all-gather.9.cloned.1.call-done) | copy-start | bytes 9437188
  257.7 5.7 %copy-start.4 = (f32[192,2]{0,1:T(2,128)S(1)}, f32[192,2]{0,1:T(2,128)}, u32[]{:S(2)}) copy-start(f32[192,2]{0,1:T(2,128)} %param.29) | copy-start | bytes 4612
  257.7 26.2 %all-to-all-start.1 = ((bf16[8,96,512]{2,1,0:T(8,128)(2,1)}), bf16[8,96,512]{2,1,0:T(8,128)(2,1)S(1)}, u32[]{:S(2)}, u32[]{:S(2)}) async-start(bf16[8,96,512]{2,1,0:T(8,128)(2,1)} %bitcast.65), calls=%async_computation.1 | async-start | bytes 1572864 | tf_op jit(solution)/shard_map/all_to_all | solution.py:152
Sparse Core Ops, SparseCore 0:
  9.5 46.9 all-gather.4
  58.7 42.5 all-gather.6
  164.6 26.5 all-gather.8
  203.0 46.3 all-gather.10
where the time goes:
time: 297 us; the launch traced here: 296 us
  waiting for transfers between devices  175 us (59%)
  blocking collectives  47.2 us (16%)
  local copies, waits for them, and re-layouts  24.5 us (8%)
  matrix products  22.8 us (8%)
  between operations  13.4 us (5%)
  starting transfers between devices  5.96 us (2%)
  other arithmetic  5.09 us (2%)
    all_gather x1, waiting for transfers between devices, local(): lax.all_gather(hidden, 'tp', axis=1, tiled=True)  46.5 us
    all_gather x1, waiting for transfers between devices, local(): value_piece = lax.all_gather(value_rows, 'sp', axis=0, tiled=True)  42.2 us
    all_gather x1, waiting for transfers between devices, local(): key_piece = lax.all_gather(key_rows, 'sp', axis=0, tiled=True)  39.5 us
    all_to_all x1, blocking collectives, local(): lax.all_to_all(outgoing, 'sp', split_axis=0, concat_axis=0, tiled=True)  32.5 us
    all_gather x1, waiting for transfers between devices, local(): lax.all_gather(lax.all_to_all(outgoing, 'sp', split_axis=0, concat_axis=0...  26.5 us
    all_to_all x1, waiting for transfers between devices, local(): lax.all_to_all(expert_out, 'sp', split_axis=0, concat_axis=0, tiled=True)  20.4 us
    unnamed x25, local copies, waits for them, and re-layouts  9.82 us
    all_gather x1, blocking collectives, local(): lax.all_gather(attended, 'tp', axis=0, tiled=True)  8.58 us
  transfers between devices with their start and end apart: 5, of which 5 were waited for; matrix products, arithmetic and copies ran while one was open for 4% of the time, Pallas kernels for 0%

commit v1 on v0

--- a/solution.py
+++ b/solution.py
@@ -62,7 +62,12 @@
     )
     folded = (empty_map, empty_map)
     key_piece = lax.all_gather(key_rows, "sp", axis=0, tiled=True)
-    value_piece = lax.all_gather(value_rows, "sp", axis=0, tiled=True)
+    ring = [value_rows]
+    for hop in range(7):
+        ring.append(lax.ppermute(ring[-1], "sp", [(dev, (dev + 1) % 8) for dev in range(8)]))
+    value_piece = jnp.roll(
+        jnp.concatenate(ring[::-1], axis=0), (lax.axis_index("sp") + 1) * ring[0].shape[0], axis=0
+    )
     key_count = key_piece.shape[0]
     key_width = math.gcd(key_count, 1024)
     blocks = key_count // key_width

time: 297 us -> 276 us (0.929)
  waiting for transfers between devices: 175 us -> 146 us
  local copies, waits for them, and re-layouts: 24.5 us -> 31 us
    ppermute x0 -> x7, waiting for transfers between devices: none -> 52.1 us  [local(): lax.ppermute(ring[-1], 'sp', [(dev, (dev + 1) % 8) for dev in range(8)])]
    all_gather x1 -> x0, waiting for transfers between devices: 42.2 us -> none  [local(): value_piece = lax.all_gather(value_rows, 'sp', axis=0, tiled=True)]
    all_gather x1, waiting for transfers between devices: 39.5 us -> 0.01 us  [local(): key_piece = lax.all_gather(key_rows, 'sp', axis=0, tiled=True)]
    unnamed x25 -> x40, local copies, waits for them, and re-layouts: 9.82 us -> 14.3 us
    ppermute x0 -> x7, starting transfers between devices: none -> 3.04 us  [local(): lax.ppermute(ring[-1], 'sp', [(dev, (dev + 1) % 8) for dev in range(8)])]
  transfers between devices with their start and end apart: 5 -> 11, of which waited for: 5 -> 10; matrix products, arithmetic and copies ran while one was open for 4% -> 7% of each run, Pallas kernels for 0% -> 0%
where the time goes in v1:
time: 276 us; the launch traced here: 275 us
  waiting for transfers between devices  146 us (53%)
  blocking collectives  44.8 us (16%)
  local copies, waits for them, and re-layouts  31 us (11%)
  matrix products  22.8 us (8%)
  between operations  13.5 us (5%)
  starting transfers between devices  8.82 us (3%)
  other arithmetic  5.76 us (2%)
    ppermute x7, waiting for transfers between devices, local(): lax.ppermute(ring[-1], 'sp', [(dev, (dev + 1) % 8) for dev in range(8)])  52.1 us
    all_gather x1, waiting for transfers between devices, local(): lax.all_gather(hidden, 'tp', axis=1, tiled=True)  46.5 us
    all_to_all x1, blocking collectives, local(): lax.all_to_all(outgoing, 'sp', split_axis=0, concat_axis=0, tiled=True)  30.1 us
    all_gather x1, waiting for transfers between devices, local(): lax.all_gather(lax.all_to_all(outgoing, 'sp', split_axis=0, concat_axis=0...  27.1 us
    all_to_all x1, waiting for transfers between devices, local(): lax.all_to_all(expert_out, 'sp', split_axis=0, concat_axis=0, tiled=True)  20.4 us
    unnamed x40, local copies, waits for them, and re-layouts  14.3 us
    all_gather x1, blocking collectives, local(): lax.all_gather(attended, 'tp', axis=0, tiled=True)  8.53 us
    dot_general x1, matrix products, local(): jnp.dot(lax.all_gather(hidden, 'tp', axis=1, tiled=True), weight_slice, p...  8.3 us
  transfers between devices with their start and end apart: 11, of which 10 were waited for; matrix products, arithmetic and copies ran while one was open for 7% of the time, Pallas kernels for 0%

profile of v1, /device:TPU:0, one launch (start us, length us, event | category | flops | bytes accessed | tf_op | source)
XLA Modules:
  0.0 275.1 jit_solution(16682509535948054810)
XLA Ops:
  6.5 1.1 copy.31
  7.7 3.0 %collective-permute-start = (bf16[192,4,128]{2,0,1:T(8,128)(2,1)S(1)}, bf16[192,4,128]{2,0,1:T(8,128)(2,1)S(1)}, u32[]{:S(2)}, u32[]{:S(2)}) collective-permute-start(bf16[192,4,128]{2,0,1:T(8,128)(2,1)S(1)} %copy.31), channel_id=1, source_target_pairs={{0,4},{4,8},{8,12},{12,16},{16,20},{20,24},{24,28},{28,0},{1,5},{5... | collective-permute-start | bytes 589832 | tf_op jit(solution)/shard_map/ppermute | solution.py:67
  10.7 1.6 copy.29
  12.4 0.8 copy.38
  13.2 0.1 eq.32
  13.3 0.1 eq.28
  13.5 0.9 reduce-window.6
  14.4 4.3 %collective-permute-done = bf16[192,4,128]{2,0,1:T(8,128)(2,1)S(1)} collective-permute-done((bf16[192,4,128]{2,0,1:T(8,128)(2,1)S(1)}, bf16[192,4,128]{2,0,1:T(8,128)(2,1)S(1)}, u32[]{:S(2)}, u32[]{:S(2)}) %collective-permute-start) | collective-permute-done | bytes 196640 | tf_op jit(solution)/shard_map/ppermute | solution.py:67
  18.6 0.7 broadcast_multiply_fusion
  19.3 10.2 %collective-permute-done.1 = bf16[192,4,128]{2,0,1:T(8,128)(2,1)S(1)} collective-permute-done((bf16[192,4,128]{2,0,1:T(8,128)(2,1)S(1)}, bf16[192,4,128]{2,0,1:T(8,128)(2,1)S(1)}, u32[]{:S(2)}, u32[]{:S(2)}) %collective-permute-start.1) | collective-permute-done | bytes 196640 | tf_op jit(solution)/shard_map/ppermute | solution.py:67
  29.5 0.2 slice_reduce_fusion
  29.7 0.1 copy.37
  29.9 0.1 mul.177
  30.0 0.1 fusion.44
  30.1 7.9 %collective-permute-done.2 = bf16[192,4,128]{2,0,1:T(8,128)(2,1)S(1)} collective-permute-done((bf16[192,4,128]{2,0,1:T(8,128)(2,1)S(1)}, bf16[192,4,128]{2,0,1:T(8,128)(2,1)S(1)}, u32[]{:S(2)}, u32[]{:S(2)}) %collective-permute-start.2) | collective-permute-done | bytes 196640 | tf_op jit(solution)/shard_map/ppermute | solution.py:67
  38.0 1.9 fusion.56
  39.9 6.6 %collective-permute-done.3 = bf16[192,4,128]{2,0,1:T(8,128)(2,1)S(1)} collective-permute-done((bf16[192,4,128]{2,0,1:T(8,128)(2,1)S(1)}, bf16[192,4,128]{2,0,1:T(8,128)(2,1)S(1)}, u32[]{:S(2)}, u32[]{:S(2)}) %collective-permute-start.3) | collective-permute-done | bytes 196640 | tf_op jit(solution)/shard_map/ppermute | solution.py:67
  46.5 12.6 %collective-permute-done.4 = bf16[192,4,128]{2,0,1:T(8,128)(2,1)S(1)} collective-permute-done((bf16[192,4,128]{2,0,1:T(8,128)(2,1)S(1)}, bf16[192,4,128]{2,0,1:T(8,128)(2,1)S(1)}, u32[]{:S(2)}, u32[]{:S(2)}) %collective-permute-start.4) | collective-permute-done | bytes 196640 | tf_op jit(solution)/shard_map/ppermute | solution.py:67
  59.1 2.9 %scatter_custom_fusion = s32[768]{0:T(1024)S(1)} fusion(s32[384]{0:T(512)S(1)} %fusion.51, s32[384]{0:T(512)S(1)} %add_select_fusion.1, s32[]{:T(128)} %constant.159.clone.1), kind=kCustom, calls=%fused_computation.106 | custom fusion | bytes 3076 | tf_op jit(solution)/shard_map/scatter | solution.py:132
  62.1 5.5 %collective-permute-done.5 = bf16[192,4,128]{2,0,1:T(8,128)(2,1)} collective-permute-done((bf16[192,4,128]{2,0,1:T(8,128)(2,1)S(1)}, bf16[192,4,128]{2,0,1:T(8,128)(2,1)}, u32[]{:S(2)}, u32[]{:S(2)}) %collective-permute-start.5) | collective-permute-done | bytes 196640 | tf_op jit(solution)/shard_map/ppermute | solution.py:67
  67.6 1.1 copy.41
  68.7 1.7 copy.42
  70.4 0.8 dynamic_slice.33
  71.1 5.1 %collective-permute-done.6 = bf16[192,4,128]{2,0,1:T(8,128)(2,1)} collective-permute-done((bf16[192,4,128]{2,0,1:T(8,128)(2,1)}, bf16[192,4,128]{2,0,1:T(8,128)(2,1)}, u32[]{:S(2)}, u32[]{:S(2)}) %collective-permute-start.6) | collective-permute-done | bytes 196640 | tf_op jit(solution)/shard_map/ppermute | solution.py:67
  76.3 0.9 constant_dynamic-update-slice_fusion.15
  77.2 1.0 constant_dynamic-update-slice_fusion.14
  78.4 1.0 constant_dynamic-update-slice_fusion.7
  79.4 1.0 constant_dynamic-update-slice_fusion.6
  80.6 0.4 constant_dynamic-slice_fusion
  81.0 1.2 copy.36
  82.3 2.6 copy.35
  85.0 8.8 %while.23 = (s32[]{:T(128)}, f32[4,192]{1,0:T(4,128)S(1)}, f32[4,192]{1,0:T(4,128)S(1)}, f32[4,192,128]{2,1,0:T(8,128)S(1)}, f32[4,192]{1,0:T(4,128)S(1)}, /*ind...) while((s32[]{:T(128)}, f32[4,192]{1,0:T(4,128)S(1)}, ...), condition=%wide.region_7.8_spmd.clone, body=%wide.region_0.7_spmd.clone.sunk | while | flops 309574784 | bytes 20891532 | solution.py:93
  85.0 0.6 dynamic_slice.48
  86.3 4.8 %conditional.3 = ((f32[4,192]{1,0:T(4,128)S(1)}, f32[4,192]{1,0:T(4,128)S(1)}, f32[4,192,128]{2,1,0:T(8,128)S(1)}, f32[4,192]{1,0:T(4,128)S(1)}, f32[4,192]{1,0:T(4,128)S(1)}, /*index=5*/f32[4,192,128]{2,1,0:T(8,128)S(1)})) conditional(s32[]{:T(128)} %convert_element_type.82, (f32[4,192]{1,0:T(4,128)S(1)}, f32[4,192]{1,0:T(4,128)S(1)}, ...), branch_computations={%region_1.1_spmd, %region_2.6_spmd.clone} | conditional | flops 309572096 | bytes 20887848 | solution.py:88
  86.4 0.1 broadcast_compare_fusion
  86.5 1.1 dynamic-slice_bitcast_fusion
  87.6 0.6 fusion.54
  88.2 0.6 fusion.55
  88.7 1.2 fusion.5
  90.0 0.6 convolution_add_fusion
  90.5 0.6 convolution_add_fusion.1
  91.2 0.6 dynamic_slice.48
  92.5 0.6 dynamic_slice.48
  93.8 0.5 multiply_reduce_fusion.2
  94.3 0.2 multiply_convert_fusion.2
  94.5 8.5 %all_gather.13 = bf16[16,192,128]{2,1,0:T(8,128)(2,1)S(1)} all-gather(bf16[4,192,128]{2,1,0:T(8,128)(2,1)S(1)} %multiply_convert_fusion.2), channel_id=1, replica_groups=mesh['sp'=8,'tp'=4] {'tp'}, dimensions={0}, use_global_device_ids=true | all-gather | bytes 983040 | tf_op jit(solution)/shard_map/all_gather | solution.py:108
  103.1 0.7 multiply_reduce_fusion.1
  103.7 6.2 %psum.7 = f32[192]{0:T(256)S(1)} all-reduce(f32[192]{0:T(256)S(1)} %get-tuple-element.467), channel_id=1, replica_groups=mesh['sp'=8,'tp'=4] {'tp'}, use_global_device_ids=true, to_apply=%region_10.11 | all-reduce | flops 192 | bytes 1536 | tf_op jit(solution)/shard_map/psum | solution.py:115
  110.0 0.1 multiply_convert_fusion.1
  110.1 2.7 gather_fusion
  112.8 30.1 %all_to_all.10 = bf16[8,96,512]{2,1,0:T(8,128)(2,1)} all-to-all(bf16[8,96,512]{2,1,0:T(8,128)(2,1)S(1)} %bitcast.63), channel_id=1, replica_groups=mesh['sp'=8,'tp'=4] {'sp'}, dimensions={0} | all-to-all | bytes 1572864 | tf_op jit(solution)/shard_map/all_to_all | solution.py:137
  142.9 0.2 all-gather.8.cloned.1.call-start
  143.1 27.1 %all-gather.6.cloned.1.call-done = bf16[8,96,2048]{2,1,0:T(8,128)(2,1)} async-done(((bf16[8,96,512]{2,1,0:T(8,128)(2,1)}), bf16[8,96,2048]{2,1,0:T(8,128)(2,1)}) %all-gather.6.cloned.1.call-update) | async-done | bytes 3145744 | tf_op jit(solution)/shard_map/all_gather | solution.py:136
  170.2 6.3 %fusion.32 = f32[768,1024]{1,0:T(8,128)S(1)} fusion(bf16[768,2048]{1,0:T(8,128)(2,1)} %bitcast.67, bf16[1,2048,1024]{2,1,0:T(8,128)(2,1)} %param.26), kind=kOutput, calls=%fused_computation.55 | convolution fusion | flops 3221225472 | bytes 10485760 | tf_op jit(solution)/shard_map/dot_general | solution.py:146
  176.5 5.3 %multiply_convert_fusion = bf16[768,1024]{1,0:T(8,128)(2,1)} fusion(f32[768,1024]{1,0:T(8,128)S(1)} %fusion.32, bf16[768,2048]{1,0:T(8,128)(2,1)S(1)} %bitcast.68, bf16[1,2048,1024]{2,1,0:T(8,128)(2,1)S(1)} %copy-done.8), kind=kOutput, calls=%fused_computation.59 | convolution fusion | flops 3229089792 | bytes 12058624 | tf_op jit(solution)/shard_map/dot_general | solution.py:145
  181.8 46.5 %all-gather.8.cloned.1.call-done = bf16[768,4096]{1,0:T(8,128)(2,1)} async-done(((bf16[768,1024]{1,0:T(8,128)(2,1)}), bf16[768,4096]{1,0:T(8,128)(2,1)}) %all-gather.8.cloned.1.call-update) | async-done | bytes 6291472 | tf_op jit(solution)/shard_map/all_gather | solution.py:152
  228.3 8.3 %fusion.38 = bf16[768,512]{1,0:T(8,128)(2,1)} fusion(bf16[768,4096]{1,0:T(8,128)(2,1)} %all-gather.8.cloned.1.call-done, bf16[1,4096,512]{2,1,0:T(8,128)(2,1)} %param.27), kind=kOutput, calls=%fused_computation.60 | convolution fusion | flops 3221618688 | bytes 11272192 | tf_op jit(solution)/shard_map/dot_general | solution.py:151
  236.6 5.5 %all-to-all-start.1 = ((bf16[8,96,512]{2,1,0:T(8,128)(2,1)}), bf16[8,96,512]{2,1,0:T(8,128)(2,1)S(1)}, u32[]{:S(2)}, u32[]{:S(2)}) async-start(bf16[8,96,512]{2,1,0:T(8,128)(2,1)} %bitcast.65), calls=%async_computation.1 | async-start | bytes 1572864 | tf_op jit(solution)/shard_map/all_to_all | solution.py:157
  242.2 0.1 copy.40
  242.3 20.4 %all-to-all-done.1 = bf16[8,96,512]{2,1,0:T(8,128)(2,1)S(1)} async-done(((bf16[8,96,512]{2,1,0:T(8,128)(2,1)}), bf16[8,96,512]{2,1,0:T(8,128)(2,1)S(1)}, u32[]{:S(2)}, u32[]{:S(2)}) %all-to-all-start.1) | async-done | bytes 786464 | tf_op jit(solution)/shard_map/all_to_all | solution.py:157
  262.7 2.6 gather_fusion.1
  265.3 1.5 reshape.153
  266.8 1.0 multiply_reduce_fusion
  267.8 0.7 add_convert_fusion
  (86 shorter events, 0.9 us)
Async XLA Ops:
  6.5 96.5 %copy-start = (bf16[2048,512]{1,0:T(8,128)(2,1)S(1)}, bf16[2048,512]{1,0:T(8,128)(2,1)}, u32[]{:S(2)}) copy-start(bf16[2048,512]{1,0:T(8,128)(2,1)} %param.23) | copy-start | bytes 6291460
  6.5 71.8 %copy-start.2 = (bf16[192,4,128]{2,1,0:T(4,128)(2,1)S(1)}, bf16[192,4,128]{2,1,0:T(4,128)(2,1)}, u32[]{:S(2)}) copy-start(bf16[192,4,128]{2,1,0:T(4,128)(2,1)} %param.20) | copy-start | bytes 589828
  6.5 75.7 %all-gather.4.cloned.1.call-start = ((), (), s32[]{:S(2)}) async-start(), calls=%async_computation.2 | async-start | bytes 1769472 | tf_op jit(solution)/shard_map/all_gather | solution.py:64
  7.7 11.0 %collective-permute-start = (bf16[192,4,128]{2,0,1:T(8,128)(2,1)S(1)}, bf16[192,4,128]{2,0,1:T(8,128)(2,1)S(1)}, u32[]{:S(2)}, u32[]{:S(2)}) collective-permute-start(bf16[192,4,128]{2,0,1:T(8,128)(2,1)S(1)} %copy.31), channel_id=1, source_target_pairs={{0,4},{4,8},{8,12},{12,16},{16,20},{20,24},{24,28},{28,0},{1,5},{5... | collective-permute-start | bytes 589832 | tf_op jit(solution)/shard_map/ppermute | solution.py:67
  12.3 157.8 %all-gather.6.cloned.1.call-start = ((), (), s32[]{:S(2)}) async-start(), calls=%async_computation.3 | async-start | bytes 3932160 | tf_op jit(solution)/shard_map/all_gather | solution.py:136
  18.6 10.8 %collective-permute-start.1 = (bf16[192,4,128]{2,0,1:T(8,128)(2,1)S(1)}, bf16[192,4,128]{2,0,1:T(8,128)(2,1)S(1)}, u32[]{:S(2)}, u32[]{:S(2)}) collective-permute-start(bf16[192,4,128]{2,0,1:T(8,128)(2,1)S(1)} %collective-permute-done), channel_id=1, source_target_pairs={{0,4},{4,8},{8,12},{12,16},{16,20},{20,24},{24,28},{28,0},{1,5},{5... | collective-permute-start | bytes 589832 | tf_op jit(solution)/shard_map/ppermute | solution.py:67
  29.5 8.5 %collective-permute-start.2 = (bf16[192,4,128]{2,0,1:T(8,128)(2,1)S(1)}, bf16[192,4,128]{2,0,1:T(8,128)(2,1)S(1)}, u32[]{:S(2)}, u32[]{:S(2)}) collective-permute-start(bf16[192,4,128]{2,0,1:T(8,128)(2,1)S(1)} %collective-permute-done.1), channel_id=1, source_target_pairs={{0,4},{4,8},{8,12},{12,16},{16,20},{20,24},{24,28},{28,0},{1,5},{5... | collective-permute-start | bytes 589832 | tf_op jit(solution)/shard_map/ppermute | solution.py:67
  38.0 8.6 %collective-permute-start.3 = (bf16[192,4,128]{2,0,1:T(8,128)(2,1)S(1)}, bf16[192,4,128]{2,0,1:T(8,128)(2,1)S(1)}, u32[]{:S(2)}, u32[]{:S(2)}) collective-permute-start(bf16[192,4,128]{2,0,1:T(8,128)(2,1)S(1)} %collective-permute-done.2), channel_id=1, source_target_pairs={{0,4},{4,8},{8,12},{12,16},{16,20},{20,24},{24,28},{28,0},{1,5},{5... | collective-permute-start | bytes 589832 | tf_op jit(solution)/shard_map/ppermute | solution.py:67
  46.5 12.6 %collective-permute-start.4 = (bf16[192,4,128]{2,0,1:T(8,128)(2,1)S(1)}, bf16[192,4,128]{2,0,1:T(8,128)(2,1)S(1)}, u32[]{:S(2)}, u32[]{:S(2)}) collective-permute-start(bf16[192,4,128]{2,0,1:T(8,128)(2,1)S(1)} %collective-permute-done.3), channel_id=1, source_target_pairs={{0,4},{4,8},{8,12},{12,16},{16,20},{20,24},{24,28},{28,0},{1,5},{5... | collective-permute-start | bytes 589832 | tf_op jit(solution)/shard_map/ppermute | solution.py:67
  59.1 8.5 %collective-permute-start.5 = (bf16[192,4,128]{2,0,1:T(8,128)(2,1)S(1)}, bf16[192,4,128]{2,0,1:T(8,128)(2,1)}, u32[]{:S(2)}, u32[]{:S(2)}) collective-permute-start(bf16[192,4,128]{2,0,1:T(8,128)(2,1)S(1)} %collective-permute-done.4), channel_id=1, source_target_pairs={{0,4},{4,8},{8,12},{12,16},{16,20},{20,24},{24,28},{28,0},{1,5},{5... | collective-permute-start | bytes 589832 | tf_op jit(solution)/shard_map/ppermute | solution.py:67
  67.6 8.7 %collective-permute-start.6 = (bf16[192,4,128]{2,0,1:T(8,128)(2,1)}, bf16[192,4,128]{2,0,1:T(8,128)(2,1)}, u32[]{:S(2)}, u32[]{:S(2)}) collective-permute-start(bf16[192,4,128]{2,0,1:T(8,128)(2,1)} %collective-permute-done.5), channel_id=1, source_target_pairs={{0,4},{4,8},{8,12},{12,16},{16,20},{20,24},{24,28},{28,0},{1,5},{5... | collective-permute-start | bytes 589832 | tf_op jit(solution)/shard_map/ppermute | solution.py:67
  81.0 4.0 %copy-start.4 = (bf16[192,4,64]{0,2,1:T(8,128)(2,1)S(1)}, bf16[192,4,64]{0,2,1:T(8,128)(2,1)}, u32[]{:S(2)}) copy-start(bf16[192,4,64]{0,2,1:T(8,128)(2,1)} %copy.42) | copy-start | bytes 294916
  85.0 8.9 %copy-start.6 = (f32[4]{0:T(128)S(1)}, f32[4]{0:T(128)}, u32[]{:S(2)}) copy-start(f32[4]{0:T(128)} %param.21) | copy-start | bytes 52
  85.0 9.4 %copy-start.7 = (f32[128]{0:T(128)S(1)}, f32[128]{0:T(128)}, u32[]{:S(2)}) copy-start(f32[128]{0:T(128)} %param.22) | copy-start | bytes 1540
  85.0 18.1 %copy-start.3 = (bf16[192,512]{1,0:T(8,128)(2,1)S(1)}, bf16[192,512]{1,0:T(8,128)(2,1)}, u32[]{:S(2)}) copy-start(bf16[192,512]{1,0:T(8,128)(2,1)} %param.17) | copy-start | bytes 589828
  88.1 1.8 copy-start.1
  142.9 85.4 %all-gather.8.cloned.1.call-start = ((), (), s32[]{:S(2)}) async-start(), calls=%async_computation.4 | async-start | bytes 7864320 | tf_op jit(solution)/shard_map/all_gather | solution.py:152
  170.2 6.3 %copy-start.8 = (bf16[1,2048,1024]{2,1,0:T(8,128)(2,1)S(1)}, bf16[1,2048,1024]{2,1,0:T(8,128)(2,1)}, u32[]{:S(2)}) copy-start(bf16[1,2048,1024]{2,1,0:T(8,128)(2,1)} %param.25) | copy-start | bytes 12582916
  170.2 6.3 %copy-start.9 = (bf16[8,96,2048]{2,1,0:T(8,128)(2,1)S(1)}, bf16[8,96,2048]{2,1,0:T(8,128)(2,1)}, u32[]{:S(2)}) copy-start(bf16[8,96,2048]{2,1,0:T(8,128)(2,1)} %all-gather.6.cloned.1.call-done) | copy-start | bytes 9437188
  181.8 60.3 %copy-start.5 = (f32[192,2]{0,1:T(2,128)S(1)}, f32[192,2]{0,1:T(2,128)}, u32[]{:S(2)}) copy-start(f32[192,2]{0,1:T(2,128)} %param.29) | copy-start | bytes 4612
  236.6 26.1 %all-to-all-start.1 = ((bf16[8,96,512]{2,1,0:T(8,128)(2,1)}), bf16[8,96,512]{2,1,0:T(8,128)(2,1)S(1)}, u32[]{:S(2)}, u32[]{:S(2)}) async-start(bf16[8,96,512]{2,1,0:T(8,128)(2,1)} %bitcast.65), calls=%async_computation.1 | async-start | bytes 1572864 | tf_op jit(solution)/shard_map/all_to_all | solution.py:157
Sparse Core Ops, SparseCore 0:
  12.5 51.5 all-gather.3
  143.0 27.1 all-gather.5
  181.9 46.3 all-gather.7
